TPU v7x, 32 devices: a whole 2x2x4 slice. The times are simulated.
32 devices in a mesh: ra: 4 (over y, x), cb: 8 (over z, core).
Axes of the slice: x: 2, y: 2, z: 4, core: 2. Of those that a mesh axis runs over, the one named last changes fastest.
Arguments:
- tokens: bfloat16 [256, 4096], P(None, 'ra'), may hold values from -20 to 20, as said below
- norm_gain: float32 [2, 4096], P(None, 'ra'), may hold values from 0.1 to 1.9
- gate_weight: bfloat16 [2, 4096, 11008], P(None, 'ra', 'cb'), may hold values from -0.09375 to 0.09375
- value_weight: bfloat16 [2, 4096, 11008], P(None, 'ra', 'cb'), may hold values from -0.09375 to 0.09375
- gate_taps: float32 [2, 3, 11008], P(None, None, 'cb'), may hold values from -3.5 to 3.5
- value_taps: float32 [2, 3, 11008], P(None, None, 'cb'), may hold values from -3.5 to 3.5
- down_weight: bfloat16 [2, 11008, 4096], P(None, 'cb', 'ra'), may hold values from -0.0546875 to 0.0546875
Outputs:
- mixed: bfloat16 [256, 4096], P(None, 'ra')
Inputs may be any that keep to these rules, and one draw needn't show every extreme that they name: tokens have features drawn around zero with a scale that varies by blocks of features between about 0.3 and 3.3.
All inputs are finite; a program needn't handle non-finite values.
Results may differ from a plain program's by a relative error of at most 0.0075.
Values may be sent and summed in bfloat16 or wider, within the bound.
No kernel may reach another device: no remote copies, remote signals or barrier semaphores. Data moves between devices by JAX's collectives and lax.ppermute only.
A program may use at most 128 MiB of HBM per device.

v0:
```python
import jax
import jax.numpy as jnp
from jax import lax
from jax.sharding import PartitionSpec as P

D = 4096
epsilon = 1e-06


def conv_after(signal, earlier, kernel_taps):
    length = signal.shape[0]
    width = kernel_taps.shape[0]
    padded = jnp.concatenate([earlier, signal], axis=0)
    result = jnp.zeros(signal.shape, jnp.float32)
    for offset in range(width):
        result = result + kernel_taps[offset] * padded[offset : offset + length]
    return result


def causal_conv(signal, kernel_taps):
    width = kernel_taps.shape[0]
    return conv_after(signal, jnp.zeros((width - 1, signal.shape[1]), jnp.float32), kernel_taps)


def body(tokens, norm_gain, gate_weight, value_weight, gate_taps, value_taps, down_weight):
    stream = tokens
    for layer_index in range(gate_weight.shape[0]):
        current = stream.astype(jnp.float32)
        local_squares = jnp.sum(current * current, axis=1, keepdims=True)
        scaled = (current * norm_gain[layer_index]).astype(jnp.bfloat16)
        gate_part = jnp.dot(scaled, gate_weight[layer_index], preferred_element_type=jnp.float32)
        value_part = jnp.dot(scaled, value_weight[layer_index], preferred_element_type=jnp.float32)
        total_squares = lax.psum(local_squares, "ra")
        gate_sum, value_sum = lax.psum((gate_part, value_part), "ra")
        inverse_rms = lax.rsqrt(total_squares / D + epsilon)
        gate_conv = causal_conv(gate_sum * inverse_rms, gate_taps[layer_index])
        value_conv = causal_conv(value_sum * inverse_rms, value_taps[layer_index])
        hidden = (jax.nn.silu(gate_conv) * value_conv).astype(jnp.bfloat16)
        partial_branch = jnp.dot(
            hidden, down_weight[layer_index], preferred_element_type=jnp.float32
        )
        branch = lax.psum(partial_branch, "cb")
        stream = (0.5 * current + branch).astype(jnp.bfloat16)
    return stream


def solution(mesh):
    return jax.shard_map(
        body,
        mesh=mesh,
        in_specs=(
            P(None, "ra"),
            P(None, "ra"),
            P(None, "ra", "cb"),
            P(None, "ra", "cb"),
            P(None, None, "cb"),
            P(None, None, "cb"),
            P(None, "cb", "ra"),
        ),
        out_specs=P(None, "ra"),
        check_vma=False,
    )
```

profile of v0, /device:TPU:0, one launch (start us, length us, event | category | flops | bytes accessed | tf_op | source)
XLA Modules:
  0.0 333.7 jit_solution(11090075387825171046)
XLA Ops:
  6.5 0.0 all-reduce.17.cloned.1.call-start
  6.5 0.8 fusion.57
  7.3 0.0 copy-start
  7.3 4.0 %fusion.8 = f32[256,1376]{0,1:T(8,128)} fusion(bf16[2,1024,1376]{1,2,0:T(8,128)(2,1)} %param.10, bf16[256,1024]{1,0:T(8,128)(2,1)} %param.7, f32[1024]{0:T(1024)S(1)} %bitcast.30), kind=kOutput, calls=%fused_computation.8 | convolution fusion | flops 722206720 | bytes 4755456 | tf_op jit(solution)/shard_map/dot_general | solution.py:32
  11.4 0.0 copy-done
  11.4 3.8 %fusion.10 = f32[256,1376]{0,1:T(8,128)} fusion(bf16[2,1024,1376]{1,2,0:T(8,128)(2,1)} %param.9, bf16[256,1024]{1,0:T(8,128)(2,1)S(1)} %copy-done, f32[1024]{0:T(1024)S(1)} %bitcast.31), kind=kOutput, calls=%fused_computation.10 | convolution fusion | flops 722206720 | bytes 4755456 | tf_op jit(solution)/shard_map/dot_general | solution.py:31
  15.2 0.0 copy-start.1
  15.2 0.0 all-reduce.17.cloned.1.call-update
  15.2 0.0 all-reduce.11.cloned.1.call-start
  15.3 0.2 fusion.41
  15.5 11.5 %psum.57 = f32[256,1]{0,1:T(1,128)S(1)} all-reduce(f32[256,1]{0,1:T(1,128)S(1)} %bitcast.27), channel_id=1, replica_groups=mesh['ra'=4,'cb'=8] {'ra'}, use_global_device_ids=true, to_apply=%region_2.0 | all-reduce | flops 256 | bytes 2048 | tf_op jit(solution)/shard_map/psum | solution.py:33
  27.0 0.0 copy-done.1
  27.0 0.0 copy-done.2
  27.0 0.2 slice_reduce_fusion.2
  27.1 72.5 %all-reduce.17.cloned.1.call-done = (f32[256,1376]{0,1:T(8,128)}, f32[256,1376]{0,1:T(8,128)}) async-done(((f32[256,1376]{0,1:T(8,128)}, f32[256,1376]{0,1:T(8,128)}), (f32[256,1376]{0,1:T(8,128)}, f32[256,1376]{0,1:T(8,128)})) %all-reduce.17.cloned.1.call-update) | async-done | bytes 2818064 | tf_op jit(solution)/shard_map/psum | solution.py:34
  99.6 2.0 broadcast_multiply_fusion.3
  101.6 6.3 %fusion.6 = f32[256,1024]{1,0:T(8,128)} fusion(bf16[2,1376,1024]{2,1,0:T(8,128)(2,1)} %param.13, f32[256,1376]{0,1:T(8,128)S(1)} %get-tuple-element.28, f32[256,1376]{0,1:T(8,128)S(1)} %get-tuple-element.27, f32[1376]{0:T(1024)S(1)} %get-tuple-element.12, f32[1376]{0:T(1024)S(1)} %get-tuple-element.13, f32[1376]{0:T(1024)S(1)} %get-tuple-element.14, ...), kind=kOutput, calls=%fused_computation.6 | convolution fusion | flops 727056384 | bytes 6717696 | tf_op jit(solution)/shard_map/dot_general | solution.py:39
  107.9 0.0 all-reduce.11.cloned.1.call-update
  107.9 0.0 all-reduce.15.cloned.1.call-start
  107.9 59.4 %all-reduce.11.cloned.1.call-done = f32[256,1024]{1,0:T(8,128)} async-done(((f32[256,1024]{1,0:T(8,128)}), f32[256,1024]{1,0:T(8,128)}) %all-reduce.11.cloned.1.call-update) | async-done | bytes 1048592 | tf_op jit(solution)/shard_map/psum | solution.py:42
  167.3 1.5 fusion.45
  168.8 3.8 %fusion.4 = f32[256,1376]{0,1:T(8,128)} fusion(bf16[2,1024,1376]{1,2,0:T(8,128)(2,1)} %param.9, bf16[256,1024]{1,0:T(8,128)(2,1)S(1)} %get-tuple-element.22, f32[1024]{0:T(1024)S(1)} %bitcast.28), kind=kOutput, calls=%fused_computation.4 | convolution fusion | flops 722206720 | bytes 4755456 | tf_op jit(solution)/shard_map/dot_general | solution.py:31
  172.6 3.8 %fusion.2 = f32[256,1376]{0,1:T(8,128)} fusion(bf16[2,1024,1376]{1,2,0:T(8,128)(2,1)} %param.10, bf16[256,1024]{1,0:T(8,128)(2,1)S(1)} %get-tuple-element.22, f32[1024]{0:T(1024)S(1)} %bitcast.29), kind=kOutput, calls=%fused_computation.2 | convolution fusion | flops 722206720 | bytes 4755456 | tf_op jit(solution)/shard_map/dot_general | solution.py:32
  176.5 0.0 all-reduce.15.cloned.1.call-update
  176.5 0.0 all-reduce.13.cloned.1.call-start
  176.5 10.1 %psum.61 = f32[256,1]{0,1:T(1,128)S(1)} all-reduce(f32[256,1]{0,1:T(1,128)S(1)} %bitcast.24), channel_id=1, replica_groups=mesh['ra'=4,'cb'=8] {'ra'}, use_global_device_ids=true, to_apply=%region_7.8 | all-reduce | flops 256 | bytes 2048 | tf_op jit(solution)/shard_map/psum | solution.py:33
  186.6 70.6 %all-reduce.15.cloned.1.call-done = (f32[256,1376]{0,1:T(8,128)}, f32[256,1376]{0,1:T(8,128)}) async-done(((f32[256,1376]{0,1:T(8,128)}, f32[256,1376]{0,1:T(8,128)}), (f32[256,1376]{0,1:T(8,128)}, f32[256,1376]{0,1:T(8,128)})) %all-reduce.15.cloned.1.call-update) | async-done | bytes 2818064 | tf_op jit(solution)/shard_map/psum | solution.py:34
  257.3 2.0 broadcast_multiply_fusion.1
  259.2 6.3 %fusion = f32[256,1024]{1,0:T(8,128)} fusion(bf16[2,1376,1024]{2,1,0:T(8,128)(2,1)} %param.13, f32[256,1376]{0,1:T(8,128)S(1)} %get-tuple-element.26, f32[256,1376]{0,1:T(8,128)S(1)} %get-tuple-element.25, f32[1376]{0:T(1024)S(1)} %get-tuple-element.15, f32[1376]{0:T(1024)S(1)} %get-tuple-element.16, f32[1376]{0:T(1024)S(1)} %get-tuple-element.11, ...), kind=kOutput, calls=%fused_computation | convolution fusion | flops 727056384 | bytes 6717696 | tf_op jit(solution)/shard_map/dot_general | solution.py:39
  265.5 0.0 all-reduce.13.cloned.1.call-update
  265.5 59.4 %all-reduce.13.cloned.1.call-done = f32[256,1024]{1,0:T(8,128)} async-done(((f32[256,1024]{1,0:T(8,128)}), f32[256,1024]{1,0:T(8,128)}) %all-reduce.13.cloned.1.call-update) | async-done | bytes 1048592 | tf_op jit(solution)/shard_map/psum | solution.py:42
  324.9 2.2 fusion.43
  (3 shorter events, 0.0 us)
Async XLA Ops:
  6.5 93.1 %all-reduce.17.cloned.1.call-start = ((), (), s32[]{:S(2)}) async-start(), calls=%async_computation.3 | async-start | bytes 5636096 | tf_op jit(solution)/shard_map/psum | solution.py:34
  7.3 4.0 %copy-start = (bf16[256,1024]{1,0:T(8,128)(2,1)S(1)}, bf16[256,1024]{1,0:T(8,128)(2,1)}, u32[]{:S(2)}) copy-start(bf16[256,1024]{1,0:T(8,128)(2,1)} %param.7) | copy-start | bytes 1572868
  15.2 11.8 %copy-start.1 = (f32[2,3,1376]{2,0,1:T(2,128)S(1)}, f32[2,3,1376]{2,0,1:T(2,128)}, u32[]{:S(2)}) copy-start(f32[2,3,1376]{2,0,1:T(2,128)} %param.12) | copy-start | bytes 99076
  15.2 11.8 %copy-start.2 = (f32[2,3,1376]{2,0,1:T(2,128)S(1)}, f32[2,3,1376]{2,0,1:T(2,128)}, u32[]{:S(2)}) copy-start(f32[2,3,1376]{2,0,1:T(2,128)} %param.11) | copy-start | bytes 99076
  15.2 152.1 %all-reduce.11.cloned.1.call-start = ((), (), s32[]{:S(2)}) async-start(), calls=%async_computation | async-start | bytes 2097152 | tf_op jit(solution)/shard_map/psum | solution.py:42
  107.9 149.4 %all-reduce.15.cloned.1.call-start = ((), (), s32[]{:S(2)}) async-start(), calls=%async_computation.2 | async-start | bytes 5636096 | tf_op jit(solution)/shard_map/psum | solution.py:34
  176.5 148.4 %all-reduce.13.cloned.1.call-start = ((), (), s32[]{:S(2)}) async-start(), calls=%async_computation.1 | async-start | bytes 2097152 | tf_op jit(solution)/shard_map/psum | solution.py:42
Sparse Core Ops, SparseCore 0:
  15.3 84.2 all-reduce.16
  108.0 59.2 all-reduce.10
  176.6 80.6 all-reduce.14
  265.6 59.2 all-reduce.12
where the time goes:
time: 334 us
  waiting for transfers between devices  262 us (78%)
  matrix products  28 us (8%)
  blocking collectives  21.6 us (6%)
  between operations  13.2 us (4%)
  other arithmetic  7.81 us (2%)
    psum x2, waiting for transfers between devices, body(): gate_sum, value_sum = lax.psum((gate_part, value_part), 'ra')  143 us
    psum x2, waiting for transfers between devices, body(): branch = lax.psum(partial_branch, 'cb')  119 us
    psum x2, blocking collectives, body(): total_squares = lax.psum(local_squares, 'ra')  21.6 us
    dot_general x2, matrix products, body(): jnp.dot(hidden, down_weight[layer_index], preferred_element_type=jnp.floa...  12.5 us
    dot_general x2, matrix products, body(): jnp.dot(scaled, value_weight[layer_index], preferred_element_type=jnp.flo...  7.86 us
    dot_general x2, matrix products, body(): jnp.dot(scaled, gate_weight[layer_index], preferred_element_type=jnp.floa...  7.65 us
  transfers between devices with their start and end apart: 4, of which 4 were waited for; matrix products, arithmetic and copies ran while one was open for 0% of the time, Pallas kernels for 0%

commit v1 on v0

--- a/solution.py
+++ b/solution.py
@@ -5,6 +5,15 @@
 
 D = 4096
 epsilon = 1e-06
+
+
+def doubling_sum(value, axis):
+    size = lax.axis_size(axis)
+    acc, hop = (value, 1)
+    while hop < size:
+        acc = acc + lax.ppermute(acc, axis, [(i, i ^ hop) for i in range(size)])
+        hop = 2 * hop
+    return acc
 
 
 def conv_after(signal, earlier, kernel_taps):
@@ -39,7 +48,7 @@
         partial_branch = jnp.dot(
             hidden, down_weight[layer_index], preferred_element_type=jnp.float32
         )
-        branch = lax.psum(partial_branch, "cb")
+        branch = doubling_sum(partial_branch, "cb")
         stream = (0.5 * current + branch).astype(jnp.bfloat16)
     return stream
 

time: 334 us -> 361 us (1.081)
  waiting for transfers between devices: 262 us -> 288 us
  starting transfers between devices: 0.13 us -> 8.24 us
  matrix products: 28 us -> 22.5 us
    ppermute x0 -> x6, waiting for transfers between devices: none -> 143 us  [doubling_sum(): acc = acc + lax.ppermute(acc, axis, [(i, i ^ hop) for i in range(size)])]
    psum x2 -> x0, waiting for transfers between devices: 119 us -> none  [body(): branch = lax.psum(partial_branch, 'cb')]
    ppermute x0 -> x6, starting transfers between devices: none -> 8.19 us  [doubling_sum(): acc = acc + lax.ppermute(acc, axis, [(i, i ^ hop) for i in range(size)])]
  transfers between devices with their start and end apart: 4 -> 8, of which waited for: 4 -> 8; matrix products, arithmetic and copies ran while one was open for 0% -> 0% of each run, Pallas kernels for 0% -> 0%
where the time goes in v1:
time: 361 us
  waiting for transfers between devices  288 us (80%)
  matrix products  22.5 us (6%)
  blocking collectives  20.7 us (6%)
  between operations  13.5 us (4%)
  starting transfers between devices  8.24 us (2%)
  other arithmetic  6.37 us (2%)
    psum x2, waiting for transfers between devices, body(): gate_sum, value_sum = lax.psum((gate_part, value_part), 'ra')  145 us
    ppermute x6, waiting for transfers between devices, doubling_sum(): acc = acc + lax.ppermute(acc, axis, [(i, i ^ hop) for i in range(size)])  143 us
    psum x2, blocking collectives, body(): total_squares = lax.psum(local_squares, 'ra')  20.7 us
    dot_general x2, matrix products, body(): jnp.dot(hidden, down_weight[layer_index], preferred_element_type=jnp.floa...  10.5 us
    ppermute x6, starting transfers between devices, doubling_sum(): acc = acc + lax.ppermute(acc, axis, [(i, i ^ hop) for i in range(size)])  8.19 us
  transfers between devices with their start and end apart: 8, of which 8 were waited for; matrix products, arithmetic and copies ran while one was open for 0% of the time, Pallas kernels for 0%

profile of v1, /device:TPU:0, one launch (start us, length us, event | category | flops | bytes accessed | tf_op | source)
XLA Modules:
  0.0 360.6 jit_solution(11903880196491729193)
XLA Ops:
  6.5 0.8 fusion.57
  7.3 4.0 %fusion.8 = f32[256,1376]{0,1:T(8,128)} fusion(bf16[2,1024,1376]{1,2,0:T(8,128)(2,1)} %param.10, bf16[256,1024]{1,0:T(8,128)(2,1)} %param.7, f32[1024]{0:T(1024)S(1)} %bitcast.30), kind=kOutput, calls=%fused_computation.8 | convolution fusion | flops 722206720 | bytes 4755456 | tf_op jit(solution)/shard_map/dot_general | solution.py:41
  11.4 3.8 %fusion.10 = f32[256,1376]{0,1:T(8,128)} fusion(bf16[2,1024,1376]{1,2,0:T(8,128)(2,1)} %param.9, bf16[256,1024]{1,0:T(8,128)(2,1)S(1)} %copy-done, f32[1024]{0:T(1024)S(1)} %bitcast.31), kind=kOutput, calls=%fused_computation.10 | convolution fusion | flops 722206720 | bytes 4755456 | tf_op jit(solution)/shard_map/dot_general | solution.py:40
  15.3 0.2 fusion.41
  15.5 11.5 %psum.43 = f32[256,1]{0,1:T(1,128)S(1)} all-reduce(f32[256,1]{0,1:T(1,128)S(1)} %bitcast.27), channel_id=1, replica_groups=mesh['ra'=4,'cb'=8] {'ra'}, use_global_device_ids=true, to_apply=%region_2.0 | all-reduce | flops 256 | bytes 2048 | tf_op jit(solution)/shard_map/psum | solution.py:42
  26.9 0.2 slice_reduce_fusion.2
  27.1 72.5 %all-reduce.11.cloned.1.call-done = (f32[256,1376]{0,1:T(8,128)}, f32[256,1376]{0,1:T(8,128)}) async-done(((f32[256,1376]{0,1:T(8,128)}, f32[256,1376]{0,1:T(8,128)}), (f32[256,1376]{0,1:T(8,128)}, f32[256,1376]{0,1:T(8,128)})) %all-reduce.11.cloned.1.call-update) | async-done | bytes 2818064 | tf_op jit(solution)/shard_map/psum | solution.py:43
  99.6 2.1 broadcast_multiply_fusion.3
  101.8 5.3 %fusion.6 = f32[256,1024]{1,0:T(8,128)S(1)} fusion(bf16[2,1376,1024]{2,1,0:T(8,128)(2,1)} %param.13, f32[256,1376]{0,1:T(8,128)S(1)} %get-tuple-element.28, f32[256,1376]{0,1:T(8,128)S(1)} %get-tuple-element.27, f32[1376]{0:T(1024)S(1)} %get-tuple-element.12, f32[1376]{0:T(1024)S(1)} %get-tuple-element.13, f32[1376]{0:T(1024)S(1)} %get-tuple-element.14, ...), kind=kOutput, calls=%fused_computation.6 | convolution fusion | flops 727056384 | bytes 6717696 | tf_op jit(solution)/shard_map/dot_general | solution.py:48
  107.1 0.1 collective-permute-start
  107.2 2.6 collective-permute-done
  109.8 0.2 add.87
  110.0 1.5 collective-permute-start.1
  111.6 23.7 %collective-permute-done.1 = f32[256,1024]{1,0:T(8,128)S(1)} collective-permute-done((f32[256,1024]{1,0:T(8,128)S(1)}, f32[256,1024]{1,0:T(8,128)S(1)}, u32[]{:S(2)}, u32[]{:S(2)}) %collective-permute-start.1) | collective-permute-done | bytes 1048608 | tf_op jit(solution)/shard_map/ppermute | solution.py:14
  135.3 0.2 add.88
  135.5 2.5 collective-permute-start.2
  137.9 45.3 %collective-permute-done.2 = f32[256,1024]{1,0:T(8,128)S(1)} collective-permute-done((f32[256,1024]{1,0:T(8,128)S(1)}, f32[256,1024]{1,0:T(8,128)S(1)}, u32[]{:S(2)}, u32[]{:S(2)}) %collective-permute-start.2) | collective-permute-done | bytes 1048608 | tf_op jit(solution)/shard_map/ppermute | solution.py:14
  183.2 0.3 fusion.45
  183.6 2.0 fusion.4
  185.6 2.0 fusion.2
  187.7 9.2 %psum.46 = f32[256,1]{0,1:T(1,128)S(1)} all-reduce(f32[256,1]{0,1:T(1,128)S(1)} %bitcast.24), channel_id=1, replica_groups=mesh['ra'=4,'cb'=8] {'ra'}, use_global_device_ids=true, to_apply=%region_6.7 | all-reduce | flops 256 | bytes 2048 | tf_op jit(solution)/shard_map/psum | solution.py:42
  196.9 72.4 %all-reduce.9.cloned.1.call-done = (f32[256,1376]{0,1:T(8,128)}, f32[256,1376]{0,1:T(8,128)}) async-done(((f32[256,1376]{0,1:T(8,128)}, f32[256,1376]{0,1:T(8,128)}), (f32[256,1376]{0,1:T(8,128)}, f32[256,1376]{0,1:T(8,128)})) %all-reduce.9.cloned.1.call-update) | async-done | bytes 2818064 | tf_op jit(solution)/shard_map/psum | solution.py:43
  269.4 2.0 broadcast_multiply_fusion.1
  271.3 5.2 %fusion = f32[256,1024]{1,0:T(8,128)S(1)} fusion(bf16[2,1376,1024]{2,1,0:T(8,128)(2,1)} %param.13, f32[256,1376]{0,1:T(8,128)S(1)} %get-tuple-element.26, f32[256,1376]{0,1:T(8,128)S(1)} %get-tuple-element.25, f32[1376]{0:T(1024)S(1)} %get-tuple-element.15, f32[1376]{0:T(1024)S(1)} %get-tuple-element.16, f32[1376]{0:T(1024)S(1)} %get-tuple-element.11, ...), kind=kOutput, calls=%fused_computation | convolution fusion | flops 727056384 | bytes 6717696 | tf_op jit(solution)/shard_map/dot_general | solution.py:48
  276.6 2.6 collective-permute-done.3
  279.3 0.2 add.97
  279.4 1.6 collective-permute-start.4
  281.0 23.7 %collective-permute-done.4 = f32[256,1024]{1,0:T(8,128)S(1)} collective-permute-done((f32[256,1024]{1,0:T(8,128)S(1)}, f32[256,1024]{1,0:T(8,128)S(1)}, u32[]{:S(2)}, u32[]{:S(2)}) %collective-permute-start.4) | collective-permute-done | bytes 1048608 | tf_op jit(solution)/shard_map/ppermute | solution.py:14
  304.7 0.2 add.98
  304.9 2.5 collective-permute-start.5
  307.3 45.3 %collective-permute-done.5 = f32[256,1024]{1,0:T(8,128)S(1)} collective-permute-done((f32[256,1024]{1,0:T(8,128)S(1)}, f32[256,1024]{1,0:T(8,128)S(1)}, u32[]{:S(2)}, u32[]{:S(2)}) %collective-permute-start.5) | collective-permute-done | bytes 1048608 | tf_op jit(solution)/shard_map/ppermute | solution.py:14
  352.7 1.1 fusion.43
  (23 shorter events, 0.2 us)
Async XLA Ops:
  6.5 93.1 %all-reduce.11.cloned.1.call-start = ((), (), s32[]{:S(2)}) async-start(), calls=%async_computation.1 | async-start | bytes 5636096 | tf_op jit(solution)/shard_map/psum | solution.py:43
  7.3 4.0 %copy-start = (bf16[256,1024]{1,0:T(8,128)(2,1)S(1)}, bf16[256,1024]{1,0:T(8,128)(2,1)}, u32[]{:S(2)}) copy-start(bf16[256,1024]{1,0:T(8,128)(2,1)} %param.7) | copy-start | bytes 1572868
  15.2 11.8 %copy-start.1 = (f32[2,3,1376]{2,0,1:T(2,128)S(1)}, f32[2,3,1376]{2,0,1:T(2,128)}, u32[]{:S(2)}) copy-start(f32[2,3,1376]{2,0,1:T(2,128)} %param.12) | copy-start | bytes 99076
  15.2 11.8 %copy-start.2 = (f32[2,3,1376]{2,0,1:T(2,128)S(1)}, f32[2,3,1376]{2,0,1:T(2,128)}, u32[]{:S(2)}) copy-start(f32[2,3,1376]{2,0,1:T(2,128)} %param.11) | copy-start | bytes 99076
  15.2 254.1 %all-reduce.9.cloned.1.call-start = ((), (), s32[]{:S(2)}) async-start(), calls=%async_computation | async-start | bytes 5636096 | tf_op jit(solution)/shard_map/psum | solution.py:43
  99.6 83.9 %slice-start = ((s8[5636096]{0:T(1024)(128)(4,1)}), s8[4194304]{0:T(1024)(128)(4,1)S(1)}, s32[]{:S(2)}) async-start(s8[5636096]{0:T(1024)(128)(4,1)} %bitcast.32), calls=%async_computation.2 | async-start | bytes 8388608
  101.8 81.8 %slice-start.1 = ((s8[5636096]{0:T(1024)(128)(4,1)}), s8[1441792]{0:T(1024)(128)(4,1)S(1)}, s32[]{:S(2)}) async-start(s8[5636096]{0:T(1024)(128)(4,1)} %bitcast.32), calls=%async_computation.3 | async-start | bytes 2883584
  107.1 2.7 collective-permute-start
  110.0 25.3 %collective-permute-start.1 = (f32[256,1024]{1,0:T(8,128)S(1)}, f32[256,1024]{1,0:T(8,128)S(1)}, u32[]{:S(2)}, u32[]{:S(2)}) collective-permute-start(f32[256,1024]{1,0:T(8,128)S(1)} %add.87), channel_id=1, source_target_pairs={{0,2},{1,3},{2,0},{3,1},{4,6},{5,7},{6,4},{7,5},{8,10},{9,11},{10,... | collective-permute-start | bytes 3145736 | tf_op jit(solution)/shard_map/ppermute | solution.py:14
  135.3 50.4 %slice-start.2 = ((s8[5636096]{0:T(1024)(128)(4,1)}), s8[4194304]{0:T(1024)(128)(4,1)S(1)}, s32[]{:S(2)}) async-start(s8[5636096]{0:T(1024)(128)(4,1)} %bitcast.34), calls=%async_computation.4 | async-start | bytes 8388608
  135.4 50.2 %slice-start.3 = ((s8[5636096]{0:T(1024)(128)(4,1)}), s8[1441792]{0:T(1024)(128)(4,1)S(1)}, s32[]{:S(2)}) async-start(s8[5636096]{0:T(1024)(128)(4,1)} %bitcast.34), calls=%async_computation.5 | async-start | bytes 2883584
  135.5 47.8 %collective-permute-start.2 = (f32[256,1024]{1,0:T(8,128)S(1)}, f32[256,1024]{1,0:T(8,128)S(1)}, u32[]{:S(2)}, u32[]{:S(2)}) collective-permute-start(f32[256,1024]{1,0:T(8,128)S(1)} %add.88), channel_id=1, source_target_pairs={{0,4},{1,5},{2,6},{3,7},{4,0},{5,1},{6,2},{7,3},{8,12},{9,13},{10,... | collective-permute-start | bytes 3145736 | tf_op jit(solution)/shard_map/ppermute | solution.py:14
  276.5 2.7 collective-permute-start.3
  279.4 25.3 %collective-permute-start.4 = (f32[256,1024]{1,0:T(8,128)S(1)}, f32[256,1024]{1,0:T(8,128)S(1)}, u32[]{:S(2)}, u32[]{:S(2)}) collective-permute-start(f32[256,1024]{1,0:T(8,128)S(1)} %add.97), channel_id=1, source_target_pairs={{0,2},{1,3},{2,0},{3,1},{4,6},{5,7},{6,4},{7,5},{8,10},{9,11},{10,... | collective-permute-start | bytes 3145736 | tf_op jit(solution)/shard_map/ppermute | solution.py:14
  304.9 47.8 %collective-permute-start.5 = (f32[256,1024]{1,0:T(8,128)S(1)}, f32[256,1024]{1,0:T(8,128)S(1)}, u32[]{:S(2)}, u32[]{:S(2)}) collective-permute-start(f32[256,1024]{1,0:T(8,128)S(1)} %add.98), channel_id=1, source_target_pairs={{0,4},{1,5},{2,6},{3,7},{4,0},{5,1},{6,2},{7,3},{8,12},{9,13},{10,... | collective-permute-start | bytes 3145736 | tf_op jit(solution)/shard_map/ppermute | solution.py:14
Sparse Core Ops, SparseCore 0:
  15.3 84.2 all-reduce.10
  187.8 81.4 all-reduce.8
